TPU v7x, 32 devices: a whole 2x2x4 slice. The times are simulated.
32 devices in a mesh: fs: 4 (over z), tp: 8 (over y, x, core).
Axes of the slice: x: 2, y: 2, z: 4, core: 2. Of those that a mesh axis runs over, the one named last changes fastest.
Arguments:
- tokens: bfloat16 [768, 2304], P('fs'), may hold values from -6 to 6
- gate_train: float32 [8, 2304, 2304], P(None, 'fs', 'tp'), may hold values from -0.125 to 0.125
- up_train: float32 [8, 2304, 2304], P(None, 'fs', 'tp'), may hold values from -0.125 to 0.125
- down_train: float32 [8, 2304, 2304], P(None, 'fs', 'tp'), may hold values from -0.125 to 0.125
- gain: float32 [2304], P('fs'), may hold values from 0.1 to 1.9
- routes: int32 [768, 2], P('fs'), may hold values from 0 to 7, all different within a row; in each aligned block of 192 rows (0 to 191, 192 to 383, ...) at most 72 rows name the same one
- route_weights: float32 [768, 2], P('fs'), may hold values from 0.1 to 1
Outputs:
- gate_new: bfloat16 [8, 2304, 2304], P('tp')
- up_new: bfloat16 [8, 2304, 2304], P('tp')
- down_new: bfloat16 [8, 2304, 2304], P('tp')
- mixed: bfloat16 [768, 2304], P('fs', 'tp')
Inputs may be any that keep to these rules, and one draw needn't show every extreme that they name: `routes`: each row names two different experts; in each aligned block of 192 rows at most 72 rows name one expert, a bound that some block reaches.
All inputs are finite; a program needn't handle non-finite values.
Results may differ from a plain program's by a relative error of at most 0.0095.
Values may be sent and summed in bfloat16 or wider, within the bound.
A program may use at most 128 MiB of HBM per device.

v0:
```python
import jax
import jax.numpy as jnp
from jax import lax
from jax.sharding import PartitionSpec as P

CAP = 72
norm_eps = 1e-06


def arrange(matrix, tp_count):
    experts, row_count, col_count = matrix.shape
    slices = tp_count // experts
    piece_width = col_count // slices
    shaped = matrix.reshape(experts, row_count, slices, piece_width)
    return shaped.transpose(0, 2, 3, 1).reshape(tp_count, piece_width, row_count)


def shards(tokens, gate_train, up_train, down_train, gain, routes, route_weights):
    tp_count = lax.axis_size("tp")
    experts = gate_train.shape[0]
    slices = tp_count // experts
    gain_column = gain[None, :, None]
    gate_round = (gate_train * gain_column).astype(jnp.bfloat16)
    up_round = (up_train * gain_column).astype(jnp.bfloat16)
    down_round = down_train.astype(jnp.bfloat16)
    moved = (
        lax.all_to_all(
            arrange(gate_round, tp_count), "tp", split_axis=0, concat_axis=1, tiled=True
        ),
        lax.all_to_all(arrange(up_round, tp_count), "tp", split_axis=0, concat_axis=1, tiled=True),
        lax.all_to_all(
            arrange(down_round, tp_count), "tp", split_axis=0, concat_axis=1, tiled=True
        ),
    )
    tokens_wide = tokens.astype(jnp.float32)
    normed = (
        tokens_wide
        * lax.rsqrt(jnp.mean(tokens_wide * tokens_wide, axis=1, keepdims=True) + norm_eps)
    ).astype(jnp.bfloat16)
    expert = lax.axis_index("tp") // slices
    matches = routes == expert
    member = jnp.any(matches, axis=1)
    slot_index = jnp.cumsum(member.astype(jnp.int32)) - 1
    marked = jnp.where(member, slot_index, -1)
    picker = (marked[None, :] == jnp.arange(CAP, dtype=jnp.int32)[:, None]).astype(jnp.bfloat16)
    chosen = jnp.dot(picker, normed, preferred_element_type=jnp.float32).astype(jnp.bfloat16)
    contract_last = (((1,), (1,)), ((), ()))
    gate_new, up_new, down_new = (
        lax.all_gather(moved[0], "fs", axis=2, tiled=True),
        lax.all_gather(moved[1], "fs", axis=2, tiled=True),
        lax.all_gather(moved[2], "fs", axis=2, tiled=True),
    )
    gate_pre = lax.dot_general(
        chosen, gate_new[0], contract_last, preferred_element_type=jnp.float32
    )
    up_pre = lax.dot_general(chosen, up_new[0], contract_last, preferred_element_type=jnp.float32)
    hidden = (jax.nn.silu(gate_pre) * up_pre).astype(jnp.bfloat16)
    partial_value = jnp.dot(hidden, down_new[0], preferred_element_type=jnp.float32).astype(
        jnp.bfloat16
    )
    labels = jnp.arange(experts, dtype=jnp.int32)
    member_all = jnp.any(routes[:, :, None] == labels[None, None, :], axis=1)
    slots_all = jnp.cumsum(member_all.astype(jnp.int32), axis=0) - 1
    slot_pair = jnp.take_along_axis(slots_all, routes, axis=1)
    flat_index = slot_pair * experts + routes
    received = lax.all_to_all(
        partial_value.reshape(CAP, tp_count, -1), "tp", split_axis=1, concat_axis=1, tiled=True
    )
    summed = jnp.sum(received.reshape(CAP, experts, slices, -1).astype(jnp.float32), axis=2)
    summed = summed.reshape(CAP * experts, -1)
    picked = jnp.take(summed, flat_index, axis=0)
    mixed = jnp.sum(route_weights[:, :, None] * picked, axis=1)
    return (gate_new, up_new, down_new, mixed.astype(jnp.bfloat16))


def solution(mesh):
    in_specs = (
        P("fs", None),
        P(None, "fs", "tp"),
        P(None, "fs", "tp"),
        P(None, "fs", "tp"),
        P("fs"),
        P("fs", None),
        P("fs", None),
    )
    out_specs = (P("tp", None, None), P("tp", None, None), P("tp", None, None), P("fs", "tp"))
    return jax.shard_map(shards, mesh=mesh, in_specs=in_specs, out_specs=out_specs, check_vma=False)
```

profile of v0, /device:TPU:1, one launch (start us, length us, event | category | flops | bytes accessed | tf_op | source)
XLA Modules:
  0.0 690.3 jit_solution(4470130244694976679)
XLA Ops:
  7.2 0.0 all-gather.4.cloned.1.call-start
  7.2 5.4 fusion.16
  12.6 40.1 %all_to_all.41 = bf16[8,288,576]{2,1,0:T(8,128)(2,1)} all-to-all(bf16[8,288,576]{2,1,0:T(8,128)(2,1)S(1)} %get-tuple-element.23), channel_id=1, replica_groups=mesh['fs'=4,'tp'=8] {'tp'}, dimensions={0} | all-to-all | bytes 5308416 | tf_op jit(solution)/shard_map/all_to_all | solution.py:27
  52.6 4.5 copy.89
  57.1 0.0 all-gather.4.cloned.1.call-update
  57.1 0.0 all-gather.6.cloned.1.call-start
  57.2 39.1 %all_to_all.42 = bf16[8,288,576]{2,1,0:T(8,128)(2,1)} all-to-all(bf16[8,288,576]{2,1,0:T(8,128)(2,1)S(1)} %get-tuple-element.22), channel_id=1, replica_groups=mesh['fs'=4,'tp'=8] {'tp'}, dimensions={0} | all-to-all | bytes 5308416 | tf_op jit(solution)/shard_map/all_to_all | solution.py:30
  96.3 4.5 copy.90
  100.8 0.0 all-gather.6.cloned.1.call-update
  100.8 0.0 all-gather.8.cloned.1.call-start
  100.9 3.0 convert_bitcast_fusion
  103.9 0.0 copy-start.1
  103.9 38.2 %all_to_all.43 = bf16[8,288,576]{2,1,0:T(8,128)(2,1)S(1)} all-to-all(bf16[8,288,576]{2,1,0:T(8,128)(2,1)S(1)} %convert_bitcast_fusion), channel_id=1, replica_groups=mesh['fs'=4,'tp'=8] {'tp'}, dimensions={0} | all-to-all | bytes 5308416 | tf_op jit(solution)/shard_map/all_to_all | solution.py:31
  142.2 3.4 copy.91
  145.5 0.0 all-gather.8.cloned.1.call-update
  145.6 0.6 reduce-window.15
  146.2 0.2 slice_reduce_fusion
  146.5 0.1 copy.93
  146.6 0.1 reshape.127
  146.7 0.1 add_bitcast_fusion
  146.8 2.7 gather_fusion.1
  149.5 0.1 reshape.130
  149.6 0.1 copy.94
  149.8 0.3 reduce-window.19
  150.1 0.1 slice.22
  150.2 0.1 slice_reduce_fusion.1
  150.3 0.3 fusion.17
  150.6 0.1 add_bitcast_fusion.1
  150.6 0.4 convolution_convert_fusion
  151.0 91.9 %all-gather.4.cloned.1.call-done = bf16[1,2304,2304]{1,2,0:T(8,128)(2,1)} async-done(((bf16[1,2304,576]{1,2,0:T(8,128)(2,1)}), bf16[1,2304,2304]{1,2,0:T(8,128)(2,1)}) %all-gather.4.cloned.1.call-update) | async-done | bytes 10616848 | tf_op jit(solution)/shard_map/all_gather | solution.py:49
  242.9 6.0 fusion.4
  249.0 180.4 %all-gather.6.cloned.1.call-done = bf16[1,2304,2304]{1,2,0:T(8,128)(2,1)} async-done(((bf16[1,2304,576]{1,2,0:T(8,128)(2,1)}), bf16[1,2304,2304]{1,2,0:T(8,128)(2,1)}) %all-gather.6.cloned.1.call-update) | async-done | bytes 10616848 | tf_op jit(solution)/shard_map/all_gather | solution.py:50
  429.4 186.4 %all-gather.8.cloned.1.call-done = bf16[1,2304,2304]{1,2,0:T(8,128)(2,1)} async-done(((bf16[1,2304,576]{1,2,0:T(8,128)(2,1)}), bf16[1,2304,2304]{1,2,0:T(8,128)(2,1)}) %all-gather.8.cloned.1.call-update) | async-done | bytes 10616848 | tf_op jit(solution)/shard_map/all_gather | solution.py:51
  615.8 11.9 %fusion.12 = bf16[72,2304]{1,0:T(8,128)(2,1)S(1)} fusion(bf16[1,2304,2304]{1,2,0:T(8,128)(2,1)} %all-gather.8.cloned.1.call-done, bf16[72,2304]{1,0:T(8,128)(2,1)S(1)} %convolution_convert_fusion, bf16[1,2304,2304]{1,2,0:T(8,128)(2,1)} %all-gather.6.cloned.1.call-done, f32[72,2304]{1,0:T(8,128)S(1)} %fusion.4), kind=kOutput, calls=%fused_computation.12 | convolution fusion | flops 1529985024 | bytes 22560768 | tf_op jit(solution)/shard_map/dot_general | solution.py:58
  627.7 0.7 reshape.112
  628.4 0.8 copy.96
  629.2 4.2 all-to-all-start.3
  633.3 0.1 copy.98
  633.5 0.1 reshape.121
  633.6 0.2 copy.95
  633.8 0.1 copy.92
  633.9 15.2 %copy.100 = bf16[1,2304,2304]{2,1,0:T(8,128)(2,1)} copy(bf16[1,2304,2304]{1,2,0:T(8,128)(2,1)} %all-gather.6.cloned.1.call-done) | data formatting | bytes 21233664
  649.1 15.2 %copy.99 = bf16[1,2304,2304]{2,1,0:T(8,128)(2,1)} copy(bf16[1,2304,2304]{1,2,0:T(8,128)(2,1)} %all-gather.4.cloned.1.call-done) | data formatting | bytes 21233664
  664.4 15.2 %copy.101 = bf16[1,2304,2304]{2,1,0:T(8,128)(2,1)} copy(bf16[1,2304,2304]{1,2,0:T(8,128)(2,1)} %all-gather.8.cloned.1.call-done) | data formatting | bytes 21233664
  679.6 0.1 copy.103
  679.6 1.7 gather_fusion
  681.4 0.3 reshape.120
  681.7 2.0 multiply_reduce_fusion
  (18 shorter events, 0.2 us)
Async XLA Ops:
  7.2 235.8 %all-gather.4.cloned.1.call-start = ((), (), s32[]{:S(2)}) async-start(), calls=%async_computation.4 | async-start | bytes 13271040 | tf_op jit(solution)/shard_map/all_gather | solution.py:49
  57.1 372.2 %all-gather.6.cloned.1.call-start = ((), (), s32[]{:S(2)}) async-start(), calls=%async_computation.5 | async-start | bytes 13271040 | tf_op jit(solution)/shard_map/all_gather | solution.py:50
  100.8 514.9 %all-gather.8.cloned.1.call-start = ((), (), s32[]{:S(2)}) async-start(), calls=%async_computation.6 | async-start | bytes 13271040 | tf_op jit(solution)/shard_map/all_gather | solution.py:51
  103.9 41.7 %copy-start.1 = (s32[192,2]{0,1:T(2,128)S(1)}, s32[192,2]{0,1:T(2,128)}, u32[]{:S(2)}) copy-start(s32[192,2]{0,1:T(2,128)} %param.12) | copy-start | bytes 4612
  146.8 3.5 copy-start
  248.9 384.8 %copy-start.2 = (f32[192,2]{0,1:T(2,128)S(1)}, f32[192,2]{0,1:T(2,128)}, u32[]{:S(2)}) copy-start(f32[192,2]{0,1:T(2,128)} %param.13) | copy-start | bytes 4612
  629.2 50.4 %all-to-all-start.3 = ((bf16[72,8,288]{2,0,1:T(8,128)(2,1)}), bf16[72,8,288]{2,0,1:T(8,128)(2,1)S(1)}, u32[]{:S(2)}, u32[]{:S(2)}) async-start(bf16[72,8,288]{2,0,1:T(8,128)(2,1)} %copy.96), calls=%async_computation.3 | async-start | bytes 884736 | tf_op jit(solution)/shard_map/all_to_all | solution.py:66
Sparse Core Ops, SparseCore 0:
  57.3 185.6 all-gather.3
  245.1 184.2 all-gather.5
  431.5 184.2 all-gather.7
where the time goes:
time: 692 us; the launch traced here: 690 us
  waiting for transfers between devices  459 us (66%)
  blocking collectives  117 us (17%)
  local copies, waits for them, and re-layouts  65.7 us (9%)
  matrix products  18.3 us (3%)
  between operations  13.9 us (2%)
  other arithmetic  11.9 us (2%)
    all_gather x1, waiting for transfers between devices, shards(): lax.all_gather(moved[2], 'fs', axis=2, tiled=True)  186 us
    all_gather x1, waiting for transfers between devices, shards(): lax.all_gather(moved[1], 'fs', axis=2, tiled=True)  180 us
    all_gather x1, waiting for transfers between devices, shards(): lax.all_gather(moved[0], 'fs', axis=2, tiled=True)  91.9 us
    unnamed x10, local copies, waits for them, and re-layouts  45.8 us
    all_to_all x1, blocking collectives, shards(): lax.all_to_all(arrange(gate_round, tp_count), 'tp', split_axis=0, concat_...  40.1 us
    all_to_all x1, blocking collectives, shards(): lax.all_to_all(arrange(up_round, tp_count), 'tp', split_axis=0, concat_ax...  39.1 us
    all_to_all x1, blocking collectives, shards(): lax.all_to_all(arrange(down_round, tp_count), 'tp', split_axis=0, concat_...  38.2 us
  transfers between devices with their start and end apart: 4, of which 3 were waited for; matrix products, arithmetic and copies ran while one was open for 10% of the time, Pallas kernels for 0%

commit v1 on v0

--- a/solution.py
+++ b/solution.py
@@ -46,7 +46,7 @@
     chosen = jnp.dot(picker, normed, preferred_element_type=jnp.float32).astype(jnp.bfloat16)
     contract_last = (((1,), (1,)), ((), ()))
     gate_new, up_new, down_new = (
-        lax.all_gather(moved[0], "fs", axis=2, tiled=True),
+        jnp.concatenate(lax.all_gather(moved[0], "fs"), axis=2),
         lax.all_gather(moved[1], "fs", axis=2, tiled=True),
         lax.all_gather(moved[2], "fs", axis=2, tiled=True),
     )

time: 692 us -> 692 us (level)
  no operation moved by 1% of the time
where the time goes in v1:
time: 692 us; the launch traced here: 690 us
  waiting for transfers between devices  459 us (66%)
  blocking collectives  117 us (17%)
  local copies, waits for them, and re-layouts  65.7 us (9%)
  matrix products  18.3 us (3%)
  between operations  13.9 us (2%)
  other arithmetic  11.9 us (2%)
    all_gather x1, waiting for transfers between devices, shards(): lax.all_gather(moved[2], 'fs', axis=2, tiled=True)  186 us
    all_gather x1, waiting for transfers between devices, shards(): lax.all_gather(moved[1], 'fs', axis=2, tiled=True)  180 us
    all_gather x1, waiting for transfers between devices, shards(): lax.all_gather(moved[0], 'fs')  91.9 us
    unnamed x10, local copies, waits for them, and re-layouts  45.8 us
    all_to_all x1, blocking collectives, shards(): lax.all_to_all(arrange(gate_round, tp_count), 'tp', split_axis=0, concat_...  40.1 us
    all_to_all x1, blocking collectives, shards(): lax.all_to_all(arrange(up_round, tp_count), 'tp', split_axis=0, concat_ax...  39.1 us
    all_to_all x1, blocking collectives, shards(): lax.all_to_all(arrange(down_round, tp_count), 'tp', split_axis=0, concat_...  38.2 us
  transfers between devices with their start and end apart: 4, of which 3 were waited for; matrix products, arithmetic and copies ran while one was open for 10% of the time, Pallas kernels for 0%

profile of v1, /device:TPU:1, one launch (start us, length us, event | category | flops | bytes accessed | tf_op | source)
XLA Modules:
  0.0 690.3 jit_solution(12122676894567847487)
XLA Ops:
  7.2 0.0 all-gather.4.cloned.1.call-start
  7.2 5.4 fusion.14
  12.6 40.1 %all_to_all.38 = bf16[8,288,576]{2,1,0:T(8,128)(2,1)} all-to-all(bf16[8,288,576]{2,1,0:T(8,128)(2,1)S(1)} %get-tuple-element.31), channel_id=1, replica_groups=mesh['fs'=4,'tp'=8] {'tp'}, dimensions={0} | all-to-all | bytes 5308416 | tf_op jit(solution)/shard_map/all_to_all | solution.py:27
  52.6 4.5 copy.111
  57.1 0.0 all-gather.4.cloned.1.call-update
  57.1 0.0 all-gather.6.cloned.1.call-start
  57.2 39.1 %all_to_all.39 = bf16[8,288,576]{2,1,0:T(8,128)(2,1)} all-to-all(bf16[8,288,576]{2,1,0:T(8,128)(2,1)S(1)} %get-tuple-element.30), channel_id=1, replica_groups=mesh['fs'=4,'tp'=8] {'tp'}, dimensions={0} | all-to-all | bytes 5308416 | tf_op jit(solution)/shard_map/all_to_all | solution.py:30
  96.3 4.5 copy.113
  100.8 0.0 all-gather.6.cloned.1.call-update
  100.8 0.0 all-gather.8.cloned.1.call-start
  100.9 3.0 convert_bitcast_fusion
  103.9 0.0 copy-start.1
  103.9 38.2 %all_to_all.40 = bf16[8,288,576]{2,1,0:T(8,128)(2,1)S(1)} all-to-all(bf16[8,288,576]{2,1,0:T(8,128)(2,1)S(1)} %convert_bitcast_fusion), channel_id=1, replica_groups=mesh['fs'=4,'tp'=8] {'tp'}, dimensions={0} | all-to-all | bytes 5308416 | tf_op jit(solution)/shard_map/all_to_all | solution.py:31
  142.2 3.4 copy.114
  145.5 0.0 all-gather.8.cloned.1.call-update
  145.6 0.6 reduce-window.15
  146.2 0.2 slice_reduce_fusion
  146.5 0.1 copy.116
  146.6 0.1 reshape.136
  146.7 0.1 add_bitcast_fusion
  146.8 2.7 gather_fusion.1
  149.5 0.1 reshape.139
  149.6 0.1 copy.117
  149.8 0.3 reduce-window.19
  150.1 0.1 slice.22
  150.2 0.1 slice_reduce_fusion.1
  150.3 0.3 fusion.15
  150.6 0.1 add_bitcast_fusion.1
  150.6 0.4 convolution_convert_fusion
  151.0 91.9 %all-gather.4.cloned.1.call-done = bf16[4,1,2304,576]{2,3,1,0:T(8,128)(2,1)} async-done(((bf16[1,1,2304,576]{2,3,1,0:T(8,128)(2,1)}), bf16[4,1,2304,576]{2,3,1,0:T(8,128)(2,1)}) %all-gather.4.cloned.1.call-update) | async-done | bytes 10616848 | tf_op jit(solution)/shard_map/all_gather | solution.py:49
  242.9 6.0 fusion.28
  249.0 180.4 %all-gather.6.cloned.1.call-done = bf16[1,2304,2304]{1,2,0:T(8,128)(2,1)} async-done(((bf16[1,2304,576]{1,2,0:T(8,128)(2,1)}), bf16[1,2304,2304]{1,2,0:T(8,128)(2,1)}) %all-gather.6.cloned.1.call-update) | async-done | bytes 10616848 | tf_op jit(solution)/shard_map/all_gather | solution.py:50
  429.4 186.4 %all-gather.8.cloned.1.call-done = bf16[1,2304,2304]{1,2,0:T(8,128)(2,1)} async-done(((bf16[1,2304,576]{1,2,0:T(8,128)(2,1)}), bf16[1,2304,2304]{1,2,0:T(8,128)(2,1)}) %all-gather.8.cloned.1.call-update) | async-done | bytes 10616848 | tf_op jit(solution)/shard_map/all_gather | solution.py:51
  615.8 11.9 %fusion.10 = bf16[72,2304]{1,0:T(8,128)(2,1)S(1)} fusion(bf16[1,2304,2304]{1,2,0:T(8,128)(2,1)} %all-gather.8.cloned.1.call-done, bf16[72,2304]{1,0:T(8,128)(2,1)S(1)} %convolution_convert_fusion, bf16[1,2304,2304]{1,2,0:T(8,128)(2,1)} %all-gather.6.cloned.1.call-done, f32[72,2304]{1,0:T(8,128)S(1)} %fusion.28), kind=kOutput, calls=%fused_computation.10 | convolution fusion | flops 1529985024 | bytes 22560768 | tf_op jit(solution)/shard_map/dot_general | solution.py:58
  627.7 0.7 reshape.121
  628.4 0.8 copy.119
  629.2 4.2 all-to-all-start.3
  633.3 0.1 copy.121
  633.5 0.1 reshape.130
  633.6 0.2 copy.118
  633.8 0.1 copy.115
  633.9 15.2 %copy.122 = bf16[1,2304,2304]{2,1,0:T(8,128)(2,1)} copy(bf16[1,2304,2304]{1,2,0:T(8,128)(2,1)} %bitcast.64) | data formatting | bytes 21233664
  649.1 15.2 %copy.123 = bf16[1,2304,2304]{2,1,0:T(8,128)(2,1)} copy(bf16[1,2304,2304]{1,2,0:T(8,128)(2,1)} %all-gather.6.cloned.1.call-done) | data formatting | bytes 21233664
  664.4 15.2 %copy.124 = bf16[1,2304,2304]{2,1,0:T(8,128)(2,1)} copy(bf16[1,2304,2304]{1,2,0:T(8,128)(2,1)} %all-gather.8.cloned.1.call-done) | data formatting | bytes 21233664
  679.6 0.1 copy.126
  679.6 1.7 gather_fusion
  681.4 0.3 reshape.129
  681.7 2.0 multiply_reduce_fusion
  (18 shorter events, 0.2 us)
Async XLA Ops:
  7.2 235.8 %all-gather.4.cloned.1.call-start = ((), (), s32[]{:S(2)}) async-start(), calls=%async_computation.4 | async-start | bytes 13271040 | tf_op jit(solution)/shard_map/all_gather | solution.py:49
  57.1 372.2 %all-gather.6.cloned.1.call-start = ((), (), s32[]{:S(2)}) async-start(), calls=%async_computation.5 | async-start | bytes 13271040 | tf_op jit(solution)/shard_map/all_gather | solution.py:50
  100.8 514.9 %all-gather.8.cloned.1.call-start = ((), (), s32[]{:S(2)}) async-start(), calls=%async_computation.6 | async-start | bytes 13271040 | tf_op jit(solution)/shard_map/all_gather | solution.py:51
  103.9 41.7 %copy-start.1 = (s32[192,2]{0,1:T(2,128)S(1)}, s32[192,2]{0,1:T(2,128)}, u32[]{:S(2)}) copy-start(s32[192,2]{0,1:T(2,128)} %param.12) | copy-start | bytes 4612
  146.8 3.5 copy-start
  248.9 384.8 %copy-start.2 = (f32[192,2]{0,1:T(2,128)S(1)}, f32[192,2]{0,1:T(2,128)}, u32[]{:S(2)}) copy-start(f32[192,2]{0,1:T(2,128)} %param.13) | copy-start | bytes 4612
  629.2 50.4 %all-to-all-start.3 = ((bf16[72,8,288]{2,0,1:T(8,128)(2,1)}), bf16[72,8,288]{2,0,1:T(8,128)(2,1)S(1)}, u32[]{:S(2)}, u32[]{:S(2)}) async-start(bf16[72,8,288]{2,0,1:T(8,128)(2,1)} %copy.119), calls=%async_computation.3 | async-start | bytes 884736 | tf_op jit(solution)/shard_map/all_to_all | solution.py:66
Sparse Core Ops, SparseCore 0:
  57.3 185.6 all-gather.3
  245.1 184.2 all-gather.5
  431.5 184.2 all-gather.7
